TPU v7x, 32 devices: a whole 2x2x4 slice. The times are simulated.
32 devices in a mesh: kv: 8 (over z, y), tp: 4 (over x, core).
Axes of the slice: x: 2, y: 2, z: 4, core: 2. Of those that a mesh axis runs over, the one named last changes fastest.
Arguments:
- hidden_rows: bfloat16 [128, 4096], P('kv', 'tp'), may hold values from -16 to 16
- carried_state: float32 [128, 524288], P('kv', 'tp'), may hold values from -6 to 6
- norm_gain: bfloat16 [4096], replicated, may hold values from 0.099609375 to 1.8984375
- w_query: bfloat16 [4096, 2048], P('kv', 'tp'), may hold values from -0.09375 to 0.09375
- w_key: bfloat16 [4096, 2048], P('kv', 'tp'), may hold values from -0.09375 to 0.09375
- w_decay: bfloat16 [4096, 2048], P('kv', 'tp'), may hold values from -0.375 to 0.375
- w_value: bfloat16 [4096, 4096], P('kv', 'tp'), may hold values from -0.09375 to 0.09375
- w_gate: bfloat16 [4096, 4096], P('kv', 'tp'), may hold values from -0.09375 to 0.09375
- decay_bias: float32 [2048], P('tp'), may hold values from -32 to 8
- head_gain: bfloat16 [256], replicated, may hold values from 0.099609375 to 1.8984375
- w_out: bfloat16 [4096, 4096], P('tp', 'kv'), may hold values from -0.09375 to 0.09375
- mlp_gain: bfloat16 [4096], P('tp'), may hold values from 0.099609375 to 1.8984375
- w_up: bfloat16 [4096, 16384], P('tp', 'kv'), may hold values from -0.09375 to 0.09375
- w_down: bfloat16 [16384, 4096], P('kv', 'tp'), may hold values from -0.046875 to 0.046875
Outputs:
- updated_rows: bfloat16 [128, 4096], P('kv', 'tp')
- new_state: float32 [128, 524288], P('kv', 'tp')
All inputs are finite; a program needn't handle non-finite values.
Results may differ from a plain program's by a relative error of at most 0.025.
Values may be sent and summed in bfloat16 or wider, within the bound.
A program may use at most 128 MiB of HBM per device.

v0:
```python
import jax
import jax.numpy as jnp
from jax import lax
from jax.sharding import PartitionSpec as P

D = 4096
DK = 128
DV = 256
epsilon = 1e-06
decay_normalizer = 16.0


def body(
    hidden_rows,
    carried_state,
    norm_gain,
    w_query,
    w_key,
    w_decay,
    w_value,
    w_gate,
    decay_bias,
    head_gain,
    w_out,
    mlp_gain,
    w_up,
    w_down,
):
    seq_rows = hidden_rows.shape[0]
    heads_here = decay_bias.shape[0] // DK
    gathered = lax.all_gather(hidden_rows, "tp", axis=1, tiled=True)
    whole_inputs = gathered.astype(jnp.float32)
    normed = (
        whole_inputs
        * lax.rsqrt(jnp.mean(whole_inputs * whole_inputs, axis=-1, keepdims=True) + epsilon)
        * norm_gain.astype(jnp.float32)
    ).astype(jnp.bfloat16)
    weights = (w_query, w_key, w_decay, w_value, w_gate)
    feature_blocks = lax.all_to_all(normed, "kv", split_axis=1, concat_axis=0, tiled=True)
    joined = jnp.concatenate(weights, axis=1)
    block_rows = feature_blocks
    summed = lax.psum_scatter(
        jnp.dot(block_rows, joined, preferred_element_type=jnp.float32).astype(jnp.bfloat16),
        "kv",
        scatter_dimension=0,
        tiled=True,
    ).astype(jnp.float32)
    projected = []
    offset = 0
    for weight in weights:
        projected.append(summed[:, offset : offset + weight.shape[1]])
        offset = offset + weight.shape[1]
    queries, keys_new, decay_pre, values, out_gate = [
        item.astype(jnp.bfloat16) for item in projected
    ]
    log_decay = jax.nn.log_sigmoid(decay_pre.astype(jnp.float32) + decay_bias) / decay_normalizer
    log_decay = log_decay.reshape(seq_rows, heads_here, DK)
    carried = carried_state.reshape(seq_rows, heads_here, DK, DV)
    key_heads = keys_new.astype(jnp.float32).reshape(seq_rows, heads_here, DK)
    value_heads = values.astype(jnp.float32).reshape(seq_rows, heads_here, DV)
    new_state = (
        jnp.exp(log_decay)[..., None] * carried + key_heads[..., None] * value_heads[..., None, :]
    )
    query_heads = queries.astype(jnp.float32).reshape(seq_rows, heads_here, DK) * DK ** (-0.5)
    head_out = jnp.einsum("bhk,bhkv->bhv", query_heads, new_state, precision=lax.Precision.HIGHEST)
    gate_heads = out_gate.astype(jnp.float32).reshape(seq_rows, heads_here, DV)
    mixed = head_out * lax.rsqrt(jnp.mean(head_out * head_out, axis=-1, keepdims=True) + epsilon)
    mixed = (mixed * head_gain.astype(jnp.float32) * jax.nn.silu(gate_heads)).astype(jnp.bfloat16)
    mixed = mixed.reshape(seq_rows, heads_here * DV)
    partial_out = jnp.dot(
        mixed, lax.all_gather(w_out, "kv", axis=1, tiled=True), preferred_element_type=jnp.float32
    ).astype(jnp.bfloat16)
    attn_out = lax.psum_scatter(
        partial_out.astype(jnp.float32).astype(jnp.bfloat16), "tp", scatter_dimension=1, tiled=True
    )
    residual = (hidden_rows.astype(jnp.float32) + attn_out.astype(jnp.float32)).astype(jnp.bfloat16)
    resid_float = residual.astype(jnp.float32)
    total_squares = lax.psum(jnp.sum(resid_float * resid_float, axis=-1), "tp")
    row_scale = lax.rsqrt(total_squares / D + epsilon)
    mlp_input = (resid_float * row_scale[:, None] * mlp_gain.astype(jnp.float32)).astype(
        jnp.bfloat16
    )
    up_partial = jnp.dot(
        lax.all_gather(mlp_input, "kv", axis=0, tiled=True),
        w_up,
        preferred_element_type=jnp.float32,
    ).astype(jnp.bfloat16)
    up_sum = lax.psum(up_partial.astype(jnp.float32).astype(jnp.bfloat16), "tp").astype(jnp.float32)
    activation = jnp.square(jax.nn.relu(up_sum)).astype(jnp.bfloat16)
    block_rows = activation
    mlp_total = lax.psum_scatter(
        jnp.dot(block_rows, w_down, preferred_element_type=jnp.float32).astype(jnp.bfloat16),
        "kv",
        scatter_dimension=0,
        tiled=True,
    )
    updated_rows = (resid_float + mlp_total.astype(jnp.float32)).astype(jnp.bfloat16)
    return (updated_rows, new_state.reshape(seq_rows, heads_here * DK * DV))


def solution(mesh):
    return jax.shard_map(
        body,
        mesh=mesh,
        in_specs=(
            P("kv", "tp"),
            P("kv", "tp"),
            P(),
            P("kv", "tp"),
            P("kv", "tp"),
            P("kv", "tp"),
            P("kv", "tp"),
            P("kv", "tp"),
            P("tp"),
            P(),
            P("tp", "kv"),
            P("tp"),
            P("tp", "kv"),
            P("kv", "tp"),
        ),
        out_specs=(P("kv", "tp"), P("kv", "tp")),
        check_vma=False,
    )
```

profile of v0, /device:TPU:0, one launch (start us, length us, event | category | flops | bytes accessed | tf_op | source)
XLA Modules:
  0.0 400.0 jit_solution(15394609910348088016)
XLA Ops:
  7.2 6.7 %all_gather.9 = bf16[16,4096]{1,0:T(8,128)(2,1)S(1)} all-gather(bf16[16,1024]{1,0:T(8,128)(2,1)} %param.14), channel_id=1, replica_groups=mesh['kv'=8,'tp'=4] {'tp'}, dimensions={1}, use_global_device_ids=true | all-gather | bytes 163840 | tf_op jit(solution)/shard_map/all_gather | solution.py:31
  14.0 0.7 convert_element_type.78
  15.5 6.2 %all-to-all-start = ((bf16[16,8,512]{2,0,1:T(8,128)(2,1)}), bf16[16,8,512]{2,0,1:T(8,128)(2,1)S(1)}, u32[]{:S(2)}, u32[]{:S(2)}) async-start(bf16[16,8,512]{2,0,1:T(8,128)(2,1)} %bitcast.37), calls=%async_computation | async-start | bytes 262144 | tf_op jit(solution)/shard_map/all_to_all | solution.py:39
  21.8 1.9 constant_dynamic-update-slice_fusion.4
  23.6 1.9 constant_dynamic-update-slice_fusion.3
  25.5 1.9 constant_dynamic-update-slice_fusion.2
  27.4 2.3 constant_dynamic-update-slice_fusion.1
  29.6 2.3 constant_dynamic-update-slice_fusion
  31.9 3.7 convolution_convert_fusion
  36.5 9.3 %copy.21 = f32[2,8,512,256]{3,2,1,0:T(8,128)} copy(f32[2,8,512,256]{3,1,2,0:T(8,128)} %bitcast.41) | data formatting | bytes 16777216
  45.7 55.1 %reduce-scatter.4.cloned.1.call-done = bf16[16,3584]{1,0:T(8,128)(2,1)} async-done(((bf16[128,3584]{1,0:T(8,128)(2,1)}), bf16[16,3584]{1,0:T(8,128)(2,1)}) %reduce-scatter.4.cloned.1.call-update) | async-done | bytes 114704 | tf_op jit(solution)/shard_map/reduce_scatter | solution.py:42
  100.8 0.8 slice_convert_fusion.1
  101.6 0.8 fusion.18
  102.5 0.7 slice_convert_fusion.2
  103.2 7.5 %fusion = f32[16,4,1,256]{3,2,1,0:T(1,128)S(1)} fusion(f32[16,4,128,1]{2,3,1,0:T(1,128)S(1)} %bitcast.47, f32[16,4,128,256]{3,2,1,0:T(8,128)} %bitcast.38, f32[16,4,128]{2,1,0:T(4,128)S(1)} %exp.21, f32[16,4,256]{2,1,0:T(4,128)S(1)} %reshape.62, f32[16,4,128]{2,1,0:T(4,128)S(1)} %reshape.61), kind=kOutput, calls=%fused_computation.1 | convolution fusion | flops 31457280 | bytes 8617984 | tf_op jit(solution)/shard_map/bhk,bhkv->bhv/dot_general | solution.py:65
  111.0 115.8 %all-gather.2.cloned.1.call-done = bf16[1024,4096]{1,0:T(8,128)(2,1)} async-done(((bf16[1024,512]{1,0:T(8,128)(2,1)}), bf16[1024,4096]{1,0:T(8,128)(2,1)}) %all-gather.2.cloned.1.call-update) | async-done | bytes 8388624 | tf_op jit(solution)/shard_map/all_gather | solution.py:71
  226.8 5.2 %convolution_convert_fusion.1 = bf16[16,4096]{1,0:T(8,128)(2,1)} fusion(bf16[16,1024]{1,0:T(8,128)(2,1)S(1)} %bitcast.46, bf16[1024,4096]{1,0:T(8,128)(2,1)} %all-gather.2.cloned.1.call-done), kind=kOutput, calls=%fused_computation.5 | convolution fusion | flops 134283264 | bytes 8552448 | tf_op jit(solution)/shard_map/dot_general | solution.py:70
  232.2 17.9 %reduce-scatter.6.cloned.1.call-done = bf16[16,1024]{1,0:T(8,128)(2,1)} async-done(((bf16[16,4096]{1,0:T(8,128)(2,1)}), bf16[16,1024]{1,0:T(8,128)(2,1)}) %reduce-scatter.6.cloned.1.call-update) | async-done | bytes 32784 | tf_op jit(solution)/shard_map/reduce_scatter | solution.py:73
  250.1 0.9 fusion.9
  250.9 5.8 %psum.14 = f32[16]{0:T(128)S(1)} all-reduce(f32[16]{0:T(128)S(1)} %fusion.9), channel_id=1, replica_groups=mesh['kv'=8,'tp'=4] {'tp'}, use_global_device_ids=true, to_apply=%region_5.6 | all-reduce | flops 16 | bytes 128 | tf_op jit(solution)/shard_map/psum | solution.py:78
  256.7 0.8 fusion.11
  257.5 31.1 %all_gather.11 = bf16[128,1024]{1,0:T(8,128)(2,1)S(1)} all-gather(bf16[16,1024]{1,0:T(8,128)(2,1)S(1)} %fusion.11), channel_id=1, replica_groups=mesh['kv'=8,'tp'=4] {'kv'}, dimensions={0}, use_global_device_ids=true | all-gather | bytes 294912 | tf_op jit(solution)/shard_map/all_gather | solution.py:84
  288.6 3.8 convolution_convert_fusion.2
  292.7 1.3 broadcast_multiply_fusion
  294.0 8.3 %copy.24 = f32[2,8,512,256]{3,1,2,0:T(8,128)} copy(f32[2,8,512,256]{3,2,1,0:T(8,128)S(1)} %bitcast.39) | data formatting | bytes 16777216
  302.2 1.2 mul.121
  303.5 8.1 %copy.23 = f32[2,8,512,256]{3,1,2,0:T(8,128)} copy(f32[2,8,512,256]{3,2,1,0:T(8,128)S(1)} %bitcast.40) | data formatting | bytes 16777216
  311.5 14.4 %all-reduce.2.cloned.1.call-done = bf16[128,2048]{1,0:T(8,128)(2,1)} async-done(((bf16[128,2048]{1,0:T(8,128)(2,1)}), bf16[128,2048]{1,0:T(8,128)(2,1)}) %all-reduce.2.cloned.1.call-update) | async-done | bytes 524304 | tf_op jit(solution)/shard_map/psum | solution.py:88
  325.9 3.8 convolution_convert_fusion.3
  329.7 12.4 %multiply_add_fusion = f32[16,131072]{1,0:T(8,128)} fusion(f32[16,131072]{1,0:T(8,128)} %bitcast.42, f32[16,131072]{1,0:T(8,128)} %bitcast.43, f32[16,131072]{1,0:T(8,128)} %param.15), kind=kLoop, calls=%fused_computation | loop fusion | flops 4194304 | bytes 33554432 | tf_op jit(solution)/shard_map/add | solution.py:62
  342.1 50.0 %reduce-scatter.8.cloned.1.call-done = bf16[16,1024]{1,0:T(8,128)(2,1)} async-done(((bf16[128,1024]{1,0:T(8,128)(2,1)}), bf16[16,1024]{1,0:T(8,128)(2,1)}) %reduce-scatter.8.cloned.1.call-update) | async-done | bytes 32784 | tf_op jit(solution)/shard_map/reduce_scatter | solution.py:91
  392.1 1.4 fusion.12
  (37 shorter events, 2.4 us)
Async XLA Ops:
  15.5 16.4 %all-to-all-start = ((bf16[16,8,512]{2,0,1:T(8,128)(2,1)}), bf16[16,8,512]{2,0,1:T(8,128)(2,1)S(1)}, u32[]{:S(2)}, u32[]{:S(2)}) async-start(bf16[16,8,512]{2,0,1:T(8,128)(2,1)} %bitcast.37), calls=%async_computation | async-start | bytes 262144 | tf_op jit(solution)/shard_map/all_to_all | solution.py:39
  21.7 79.1 %reduce-scatter.4.cloned.1.call-start = ((), (), s32[]{:S(2)}) async-start(), calls=%async_computation.4 | async-start | bytes 1032192 | tf_op jit(solution)/shard_map/reduce_scatter | solution.py:42
  35.6 191.2 %all-gather.2.cloned.1.call-start = ((), (), s32[]{:S(2)}) async-start(), calls=%async_computation.5 | async-start | bytes 9437184 | tf_op jit(solution)/shard_map/all_gather | solution.py:71
  36.4 213.7 %reduce-scatter.6.cloned.1.call-start = ((), (), s32[]{:S(2)}) async-start(), calls=%async_computation.6 | async-start | bytes 163840 | tf_op jit(solution)/shard_map/reduce_scatter | solution.py:73
  36.4 9.3 %copy-start.4 = (bf16[256]{0:T(256)(128)(2,1)S(1)}, bf16[256]{0:T(256)(128)(2,1)}, u32[]{:S(2)}) copy-start(bf16[256]{0:T(256)(128)(2,1)} %param.23) | copy-start | bytes 1540
  36.4 65.2 %copy-start.2 = (f32[512]{0:T(512)S(1)}, f32[512]{0:T(512)}, u32[]{:S(2)}) copy-start(f32[512]{0:T(512)} %param.22) | copy-start | bytes 6148
  110.8 121.4 %copy-start.3 = (bf16[1024]{0:T(1024)(128)(2,1)S(1)}, bf16[1024]{0:T(1024)(128)(2,1)}, u32[]{:S(2)}) copy-start(bf16[1024]{0:T(1024)(128)(2,1)} %param.25) | copy-start | bytes 6148
  110.8 139.3 %copy-start = (bf16[16,1024]{1,0:T(8,128)(2,1)S(1)}, bf16[16,1024]{1,0:T(8,128)(2,1)}, u32[]{:S(2)}) copy-start(bf16[16,1024]{1,0:T(8,128)(2,1)} %param.14) | copy-start | bytes 98308
  232.1 93.8 %all-reduce.2.cloned.1.call-start = ((), (), s32[]{:S(2)}) async-start(), calls=%async_computation.7 | async-start | bytes 1048576 | tf_op jit(solution)/shard_map/psum | solution.py:88
  292.5 99.6 %reduce-scatter.8.cloned.1.call-start = ((), (), s32[]{:S(2)}) async-start(), calls=%async_computation.8 | async-start | bytes 294912 | tf_op jit(solution)/shard_map/reduce_scatter | solution.py:91
  329.7 62.4 %copy-start.1 = (bf16[16,1024]{1,0:T(8,128)(2,1)S(1)}, bf16[16,1024]{1,0:T(8,128)(2,1)}, u32[]{:S(2)}) copy-start(bf16[16,1024]{1,0:T(8,128)(2,1)} %reduce-scatter.6.cloned.1.call-done) | copy-start | bytes 98308
Sparse Core Ops, SparseCore 0:
  35.8 65.0 reduce-scatter.3
  102.8 123.9 all-gather.1
  232.2 17.7 reduce-scatter.5
  292.6 33.2 all-reduce.1
  329.8 62.2 reduce-scatter.7
where the time goes:
time: 401 us; the launch traced here: 400 us
  waiting for transfers between devices  254 us (63%)
  blocking collectives  43.6 us (11%)
  local copies, waits for them, and re-layouts  37.8 us (9%)
  matrix products  24.1 us (6%)
  other arithmetic  20.2 us (5%)
  between operations  13.9 us (3%)
  starting transfers between devices  6.6 us (2%)
    all_gather x1, waiting for transfers between devices, body(): lax.all_gather(w_out, 'kv', axis=1, tiled=True)  116 us
    reduce_scatter x1, waiting for transfers between devices, body(): lax.psum_scatter(jnp.dot(block_rows, joined, preferred_element_type=jnp.f...  55.1 us
    reduce_scatter x1, waiting for transfers between devices, body(): lax.psum_scatter(jnp.dot(block_rows, w_down, preferred_element_type=jnp.f...  50 us
    unnamed x18, local copies, waits for them, and re-layouts  33.5 us
    all_gather x1, blocking collectives, body(): lax.all_gather(mlp_input, 'kv', axis=0, tiled=True)  31.1 us
    reduce_scatter x1, waiting for transfers between devices, body(): lax.psum_scatter(partial_out.astype(jnp.float32).astype(jnp.bfloat16), 't...  17.9 us
    psum x1, waiting for transfers between devices, body(): lax.psum(up_partial.astype(jnp.float32).astype(jnp.bfloat16), 'tp')  14.4 us
    add x1, other arithmetic, body(): jnp.exp(log_decay)[..., None] * carried  12.4 us
  transfers between devices with their start and end apart: 6, of which 5 were waited for; matrix products, arithmetic and copies ran while one was open for 15% of the time, Pallas kernels for 0%

commit v1 on v0

--- a/solution.py
+++ b/solution.py
@@ -8,6 +8,11 @@
 DV = 256
 epsilon = 1e-06
 decay_normalizer = 16.0
+
+
+def step_on_cycles(x0, named_axis):
+    y_new = jnp.concatenate(lax.all_gather(x0, named_axis), axis=1)
+    return y_new
 
 
 def body(
@@ -68,7 +73,7 @@
     mixed = (mixed * head_gain.astype(jnp.float32) * jax.nn.silu(gate_heads)).astype(jnp.bfloat16)
     mixed = mixed.reshape(seq_rows, heads_here * DV)
     partial_out = jnp.dot(
-        mixed, lax.all_gather(w_out, "kv", axis=1, tiled=True), preferred_element_type=jnp.float32
+        mixed, step_on_cycles(w_out, "kv"), preferred_element_type=jnp.float32
     ).astype(jnp.bfloat16)
     attn_out = lax.psum_scatter(
         partial_out.astype(jnp.float32).astype(jnp.bfloat16), "tp", scatter_dimension=1, tiled=True

time: 401 us -> 413 us (1.030)
  local copies, waits for them, and re-layouts: 37.8 us -> 49.1 us
    reshape x0 -> x1, local copies, waits for them, and re-layouts: none -> 11.4 us  [step_on_cycles(): y_new = jnp.concatenate(lax.all_gather(x0, named_axis), axis=1)]
where the time goes in v1:
time: 413 us; the launch traced here: 412 us
  waiting for transfers between devices  253 us (61%)
  local copies, waits for them, and re-layouts  49.1 us (12%)
  blocking collectives  43.6 us (11%)
  matrix products  25.2 us (6%)
  other arithmetic  20.2 us (5%)
  between operations  13.9 us (3%)
  starting transfers between devices  6.6 us (2%)
    all_gather x1, waiting for transfers between devices, step_on_cycles(): y_new = jnp.concatenate(lax.all_gather(x0, named_axis), axis=1)  115 us
    reduce_scatter x1, waiting for transfers between devices, body(): lax.psum_scatter(jnp.dot(block_rows, joined, preferred_element_type=jnp.f...  55.1 us
    reduce_scatter x1, waiting for transfers between devices, body(): lax.psum_scatter(jnp.dot(block_rows, w_down, preferred_element_type=jnp.f...  50 us
    unnamed x18, local copies, waits for them, and re-layouts  33.5 us
    all_gather x1, blocking collectives, body(): lax.all_gather(mlp_input, 'kv', axis=0, tiled=True)  31.1 us
    reduce_scatter x1, waiting for transfers between devices, body(): lax.psum_scatter(partial_out.astype(jnp.float32).astype(jnp.bfloat16), 't...  17.9 us
    psum x1, waiting for transfers between devices, body(): lax.psum(up_partial.astype(jnp.float32).astype(jnp.bfloat16), 'tp')  14.3 us
    add x1, other arithmetic, body(): jnp.exp(log_decay)[..., None] * carried  12.4 us
  transfers between devices with their start and end apart: 6, of which 5 were waited for; matrix products, arithmetic and copies ran while one was open for 15% of the time, Pallas kernels for 0%

profile of v1, /device:TPU:0, one launch (start us, length us, event | category | flops | bytes accessed | tf_op | source)
XLA Modules:
  0.0 412.1 jit_solution(9366324042291345289)
XLA Ops:
  7.2 6.7 %all_gather.12 = bf16[16,4096]{1,0:T(8,128)(2,1)S(1)} all-gather(bf16[16,1024]{1,0:T(8,128)(2,1)} %param.14), channel_id=1, replica_groups=mesh['kv'=8,'tp'=4] {'tp'}, dimensions={1}, use_global_device_ids=true | all-gather | bytes 163840 | tf_op jit(solution)/shard_map/all_gather | solution.py:36
  15.5 6.2 %all-to-all-start = ((bf16[16,8,512]{2,0,1:T(8,128)(2,1)}), bf16[16,8,512]{2,0,1:T(8,128)(2,1)S(1)}, u32[]{:S(2)}, u32[]{:S(2)}) async-start(bf16[16,8,512]{2,0,1:T(8,128)(2,1)} %bitcast.41), calls=%async_computation | async-start | bytes 262144 | tf_op jit(solution)/shard_map/all_to_all | solution.py:44
  21.8 1.9 constant_dynamic-update-slice_fusion.4
  23.6 1.9 constant_dynamic-update-slice_fusion.3
  25.5 1.9 constant_dynamic-update-slice_fusion.2
  27.4 2.3 constant_dynamic-update-slice_fusion.1
  29.6 2.3 constant_dynamic-update-slice_fusion
  31.9 3.7 convolution_convert_fusion
  36.5 9.3 %copy.23 = f32[2,8,512,256]{3,2,1,0:T(8,128)} copy(f32[2,8,512,256]{3,1,2,0:T(8,128)} %bitcast.46) | data formatting | bytes 16777216
  45.7 55.1 %reduce-scatter.4.cloned.1.call-done = bf16[16,3584]{1,0:T(8,128)(2,1)} async-done(((bf16[128,3584]{1,0:T(8,128)(2,1)}), bf16[16,3584]{1,0:T(8,128)(2,1)}) %reduce-scatter.4.cloned.1.call-update) | async-done | bytes 114704 | tf_op jit(solution)/shard_map/reduce_scatter | solution.py:47
  100.8 0.8 slice_convert_fusion.1
  101.6 0.8 fusion.18
  102.5 0.7 slice_convert_fusion.2
  103.2 7.5 %fusion = f32[16,4,1,256]{3,2,1,0:T(1,128)S(1)} fusion(f32[16,4,128,1]{2,3,1,0:T(1,128)S(1)} %bitcast.52, f32[16,4,128,256]{3,2,1,0:T(8,128)} %bitcast.42, f32[16,4,128]{2,1,0:T(4,128)S(1)} %exp.21, f32[16,4,256]{2,1,0:T(4,128)S(1)} %reshape.70, f32[16,4,128]{2,1,0:T(4,128)S(1)} %reshape.69), kind=kOutput, calls=%fused_computation.1 | convolution fusion | flops 31457280 | bytes 8617984 | tf_op jit(solution)/shard_map/bhk,bhkv->bhv/dot_general | solution.py:70
  111.0 115.5 %all-gather.3.cloned.1.call-done = bf16[8192,512]{1,0:T(8,128)(2,1)} async-done(((bf16[1024,512]{1,0:T(8,128)(2,1)}), bf16[8192,512]{1,0:T(8,128)(2,1)}) %all-gather.3.cloned.1.call-update) | async-done | bytes 8388624 | tf_op jit(solution)/shard_map/all_gather | solution.py:14
  226.5 11.4 %copy.19 = bf16[1024,8,512]{0,2,1:T(8,128)(2,1)} copy(bf16[1024,8,512]{2,0,1:T(8,128)(2,1)} %bitcast.49) | data formatting | bytes 16777216 | tf_op jit(solution)/shard_map/reshape | solution.py:14
  237.8 6.3 %convolution_convert_fusion.1 = bf16[16,4096]{1,0:T(8,128)(2,1)} fusion(bf16[16,1024]{1,0:T(8,128)(2,1)S(1)} %bitcast.53, bf16[1024,4096]{0,1:T(8,128)(2,1)} %bitcast.43), kind=kOutput, calls=%fused_computation.5 | convolution fusion | flops 134283264 | bytes 8552448 | tf_op jit(solution)/shard_map/dot_general | solution.py:75
  244.2 17.9 %reduce-scatter.6.cloned.1.call-done = bf16[16,1024]{1,0:T(8,128)(2,1)} async-done(((bf16[16,4096]{1,0:T(8,128)(2,1)}), bf16[16,1024]{1,0:T(8,128)(2,1)}) %reduce-scatter.6.cloned.1.call-update) | async-done | bytes 32784 | tf_op jit(solution)/shard_map/reduce_scatter | solution.py:78
  262.2 0.9 fusion.9
  263.0 5.8 %psum.14 = f32[16]{0:T(128)S(1)} all-reduce(f32[16]{0:T(128)S(1)} %fusion.9), channel_id=1, replica_groups=mesh['kv'=8,'tp'=4] {'tp'}, use_global_device_ids=true, to_apply=%region_5.6 | all-reduce | flops 16 | bytes 128 | tf_op jit(solution)/shard_map/psum | solution.py:83
  268.8 0.8 fusion.11
  269.6 31.1 %all_gather.15 = bf16[128,1024]{1,0:T(8,128)(2,1)S(1)} all-gather(bf16[16,1024]{1,0:T(8,128)(2,1)S(1)} %fusion.11), channel_id=1, replica_groups=mesh['kv'=8,'tp'=4] {'kv'}, dimensions={0}, use_global_device_ids=true | all-gather | bytes 294912 | tf_op jit(solution)/shard_map/all_gather | solution.py:89
  300.8 3.8 convolution_convert_fusion.2
  304.8 1.3 broadcast_multiply_fusion
  306.1 8.3 %copy.26 = f32[2,8,512,256]{3,1,2,0:T(8,128)} copy(f32[2,8,512,256]{3,2,1,0:T(8,128)S(1)} %bitcast.44) | data formatting | bytes 16777216
  314.4 1.2 mul.121
  315.6 8.1 %copy.25 = f32[2,8,512,256]{3,1,2,0:T(8,128)} copy(f32[2,8,512,256]{3,2,1,0:T(8,128)S(1)} %bitcast.45) | data formatting | bytes 16777216
  323.7 14.3 %all-reduce.2.cloned.1.call-done = bf16[128,2048]{1,0:T(8,128)(2,1)} async-done(((bf16[128,2048]{1,0:T(8,128)(2,1)}), bf16[128,2048]{1,0:T(8,128)(2,1)}) %all-reduce.2.cloned.1.call-update) | async-done | bytes 524304 | tf_op jit(solution)/shard_map/psum | solution.py:93
  338.0 3.8 convolution_convert_fusion.3
  341.8 12.4 %multiply_add_fusion = f32[16,131072]{1,0:T(8,128)} fusion(f32[16,131072]{1,0:T(8,128)} %bitcast.47, f32[16,131072]{1,0:T(8,128)} %bitcast.48, f32[16,131072]{1,0:T(8,128)} %param.15), kind=kLoop, calls=%fused_computation | loop fusion | flops 4194304 | bytes 33554432 | tf_op jit(solution)/shard_map/add | solution.py:67
  354.2 50.0 %reduce-scatter.8.cloned.1.call-done = bf16[16,1024]{1,0:T(8,128)(2,1)} async-done(((bf16[128,1024]{1,0:T(8,128)(2,1)}), bf16[16,1024]{1,0:T(8,128)(2,1)}) %reduce-scatter.8.cloned.1.call-update) | async-done | bytes 32784 | tf_op jit(solution)/shard_map/reduce_scatter | solution.py:96
  404.2 1.4 fusion.12
  (38 shorter events, 3.1 us)
Async XLA Ops:
  15.5 16.4 %all-to-all-start = ((bf16[16,8,512]{2,0,1:T(8,128)(2,1)}), bf16[16,8,512]{2,0,1:T(8,128)(2,1)S(1)}, u32[]{:S(2)}, u32[]{:S(2)}) async-start(bf16[16,8,512]{2,0,1:T(8,128)(2,1)} %bitcast.41), calls=%async_computation | async-start | bytes 262144 | tf_op jit(solution)/shard_map/all_to_all | solution.py:44
  21.7 79.1 %reduce-scatter.4.cloned.1.call-start = ((), (), s32[]{:S(2)}) async-start(), calls=%async_computation.4 | async-start | bytes 1032192 | tf_op jit(solution)/shard_map/reduce_scatter | solution.py:47
  35.6 190.8 %all-gather.3.cloned.1.call-start = ((), (), s32[]{:S(2)}) async-start(), calls=%async_computation.8 | async-start | bytes 9437184 | tf_op jit(solution)/shard_map/all_gather | solution.py:14
  36.4 225.8 %reduce-scatter.6.cloned.1.call-start = ((), (), s32[]{:S(2)}) async-start(), calls=%async_computation.5 | async-start | bytes 163840 | tf_op jit(solution)/shard_map/reduce_scatter | solution.py:78
  36.4 9.3 %copy-start.4 = (bf16[256]{0:T(256)(128)(2,1)S(1)}, bf16[256]{0:T(256)(128)(2,1)}, u32[]{:S(2)}) copy-start(bf16[256]{0:T(256)(128)(2,1)} %param.23) | copy-start | bytes 1540
  36.4 65.2 %copy-start.2 = (f32[512]{0:T(512)S(1)}, f32[512]{0:T(512)}, u32[]{:S(2)}) copy-start(f32[512]{0:T(512)} %param.22) | copy-start | bytes 6148
  237.8 6.4 %copy-start.3 = (bf16[1024]{0:T(1024)(128)(2,1)S(1)}, bf16[1024]{0:T(1024)(128)(2,1)}, u32[]{:S(2)}) copy-start(bf16[1024]{0:T(1024)(128)(2,1)} %param.25) | copy-start | bytes 6148
  237.8 24.3 %copy-start = (bf16[16,1024]{1,0:T(8,128)(2,1)S(1)}, bf16[16,1024]{1,0:T(8,128)(2,1)}, u32[]{:S(2)}) copy-start(bf16[16,1024]{1,0:T(8,128)(2,1)} %param.14) | copy-start | bytes 98308
  244.2 93.8 %all-reduce.2.cloned.1.call-start = ((), (), s32[]{:S(2)}) async-start(), calls=%async_computation.6 | async-start | bytes 1048576 | tf_op jit(solution)/shard_map/psum | solution.py:93
  304.6 99.6 %reduce-scatter.8.cloned.1.call-start = ((), (), s32[]{:S(2)}) async-start(), calls=%async_computation.7 | async-start | bytes 294912 | tf_op jit(solution)/shard_map/reduce_scatter | solution.py:96
  341.8 62.4 %copy-start.1 = (bf16[16,1024]{1,0:T(8,128)(2,1)S(1)}, bf16[16,1024]{1,0:T(8,128)(2,1)}, u32[]{:S(2)}) copy-start(bf16[16,1024]{1,0:T(8,128)(2,1)} %reduce-scatter.6.cloned.1.call-done) | copy-start | bytes 98308
Sparse Core Ops, SparseCore 0:
  35.8 65.0 reduce-scatter.3
  102.9 123.4 all-gather.2
  244.3 17.8 reduce-scatter.5
  304.7 33.2 all-reduce.1
  341.9 62.1 reduce-scatter.7
